TPU v7x, 32 devices: a whole 2x2x4 slice. The times are simulated.
32 devices in a mesh: sp: 4 (over y, x), tp: 8 (over z, core).
Axes of the slice: x: 2, y: 2, z: 4, core: 2. Of those that a mesh axis runs over, the one named last changes fastest.
Arguments:
- out_gate: bfloat16 [2048, 2048], P('sp', 'tp'), may hold values from -6 to 6
- in_gate: bfloat16 [2048, 2048], P('sp', 'tp'), may hold values from -6 to 6
- conv_input: bfloat16 [2048, 2048], P('sp', 'tp'), may hold values from -6 to 6
- conv_taps: bfloat16 [3, 2048], P(None, 'tp'), may hold values from -3.5 to 3.5
- documents: int32 [2048], P('sp'), may hold values from 0 to 2, never falling along the last dimension, each value on 1 to 1536 neighbouring positions
- out_weight: bfloat16 [2048, 2048], P('tp'), may hold values from -0.125 to 0.125
- residual: bfloat16 [2048, 2048], P(('sp', 'tp')), may hold values from -6 to 6
- norm_gain: bfloat16 [2048], replicated, may hold values from 0.099609375 to 1.8984375
- expert_ids: int32 [2048, 2], P(('sp', 'tp')), may hold values from 0 to 3, all different within a row; in each aligned block of 64 rows (0 to 63, 64 to 127, ...) at most 48 rows name the same one
- route_weights: float32 [2048, 2], P(('sp', 'tp')), may hold values from 0.1 to 1
- gate_weight: bfloat16 [4, 2048, 4096], P('sp', None, 'tp'), may hold values from -0.125 to 0.125
- up_weight: bfloat16 [4, 2048, 4096], P('sp', None, 'tp'), may hold values from -0.125 to 0.125
- down_weight: bfloat16 [4, 4096, 2048], P('sp', 'tp'), may hold values from -0.09375 to 0.09375
Outputs:
- layer_out: bfloat16 [2048, 2048], P(('sp', 'tp'))
Inputs may be any that keep to these rules, and one draw needn't show every extreme that they name: `expert_ids`: A token's two experts differ; in each aligned block of 64 rows no expert is named by more than 48 entries, a bound that some block reaches. `documents`: document numbers never fall along the sequence; a document holds at most 1536 positions.
All inputs are finite; a program needn't handle non-finite values.
Results may differ from a plain program's by a relative error of at most 0.017.
Values may be sent and summed in bfloat16 or wider, within the bound.
A program may use at most 64 MiB of HBM per device.

v0:
```python
import jax
import jax.numpy as jnp
from jax import lax
from jax.sharding import PartitionSpec as P

EPS = 1e-06


def passed_along(block, axis, distance):
    devices = range(lax.axis_size(axis))
    route = [(i - distance, i) for i in devices if i - distance in devices]
    return lax.ppermute(block, axis, route)


def slot_index(expert_ids, experts, capacity):
    listed = expert_ids.reshape(-1)
    onehot = (listed[:, None] == jnp.arange(experts, dtype=jnp.int32)[None, :]).astype(jnp.int32)
    earlier = jnp.cumsum(onehot, axis=0) - onehot
    within = jnp.sum(earlier * onehot, axis=1)
    return listed * capacity + within


def shards(
    out_gate,
    in_gate,
    conv_input,
    conv_taps,
    documents,
    out_weight,
    residual,
    norm_gain,
    expert_ids,
    route_weights,
    gate_weight,
    up_weight,
    down_weight,
):
    length = conv_input.shape[0]
    signal = in_gate.astype(jnp.float32) * conv_input.astype(jnp.float32)
    doc_values = documents.astype(jnp.float32)
    prior_signal, prior_docs = passed_along(
        (signal[length - 2 :], doc_values[length - 2 :]), "sp", 1
    )
    long_signal = jnp.concatenate([prior_signal, signal], axis=0)
    long_docs = jnp.concatenate([prior_docs, doc_values], axis=0)
    position = lax.axis_index("sp") * length + jnp.arange(length, dtype=jnp.int32)
    tap_values = conv_taps.astype(jnp.float32)
    mixed_conv = tap_values[2][None, :] * signal
    for offset in (1, 2):
        earlier_signal = long_signal[2 - offset : 2 - offset + length]
        earlier_docs = long_docs[2 - offset : 2 - offset + length]
        allowed = (position >= offset) & (earlier_docs == doc_values)
        mixed_conv = mixed_conv + jnp.where(
            allowed[:, None], tap_values[2 - offset][None, :] * earlier_signal, 0.0
        )
    gated = (out_gate.astype(jnp.float32) * mixed_conv).astype(jnp.bfloat16)
    block_rows = length // lax.axis_size("tp")
    mixed = lax.psum_scatter(
        jnp.dot(gated, out_weight, preferred_element_type=jnp.float32).astype(jnp.bfloat16),
        "tp",
        scatter_dimension=0,
        tiled=True,
    ).astype(jnp.float32)
    hidden_wide = (residual.astype(jnp.float32) + mixed).astype(jnp.bfloat16).astype(jnp.float32)
    stats = jnp.mean(hidden_wide * hidden_wide, axis=-1, keepdims=True)
    normed = (hidden_wide * lax.rsqrt(stats + EPS) * norm_gain.astype(jnp.float32)[None, :]).astype(
        jnp.bfloat16
    )
    model_width = normed.shape[1]
    experts = lax.axis_size("sp")
    capacity = max(2, (3 * block_rows + experts - 1) // experts)
    target = slot_index(expert_ids, experts, capacity)
    slots = jnp.arange(experts * capacity, dtype=jnp.int32)
    table = jnp.sum(
        (target.reshape(block_rows, 2)[:, :, None] == slots[None, None, :]).astype(jnp.bfloat16),
        axis=1,
    )
    outgoing = lax.dot_general(
        table, normed, (((0,), (0,)), ((), ())), preferred_element_type=jnp.float32
    ).astype(jnp.bfloat16)
    arrived = lax.all_to_all(outgoing, "sp", split_axis=0, concat_axis=0, tiled=True)
    gathered = lax.all_gather(arrived, "tp", axis=0, tiled=True)
    gate_proj = jnp.dot(gathered, gate_weight[0], preferred_element_type=jnp.float32)
    up_proj = jnp.dot(gathered, up_weight[0], preferred_element_type=jnp.float32)
    act = (jax.nn.silu(gate_proj) * up_proj).astype(jnp.bfloat16)
    summed = lax.psum_scatter(
        jnp.dot(act, down_weight[0], preferred_element_type=jnp.float32).astype(jnp.bfloat16),
        "tp",
        scatter_dimension=0,
        tiled=True,
    )
    returned = lax.all_to_all(summed, "sp", split_axis=0, concat_axis=0, tiled=True)
    picked = returned[target].astype(jnp.float32).reshape(block_rows, 2, model_width)
    combined = jnp.sum(picked * route_weights[:, :, None], axis=1)
    return (hidden_wide + combined).astype(jnp.bfloat16)


def solution(mesh):
    in_specs = (
        P("sp", "tp"),
        P("sp", "tp"),
        P("sp", "tp"),
        P(None, "tp"),
        P("sp"),
        P("tp", None),
        P(("sp", "tp"), None),
        P(),
        P(("sp", "tp"), None),
        P(("sp", "tp"), None),
        P("sp", None, "tp"),
        P("sp", None, "tp"),
        P("sp", "tp", None),
    )
    out_specs = P(("sp", "tp"), None)
    return jax.shard_map(shards, mesh=mesh, in_specs=in_specs, out_specs=out_specs, check_vma=False)
```

profile of v0, /device:TPU:0, one launch (start us, length us, event | category | flops | bytes accessed | tf_op | source)
XLA Modules:
  0.0 253.9 jit_solution(859070337036209442)
XLA Ops:
  6.5 0.8 convert_element_type.71
  7.4 4.9 %collective-permute-start = (f32[2]{0:T(128)S(1)}, f32[2]{0:T(128)S(1)}, u32[]{:S(2)}, u32[]{:S(2)}) collective-permute-start(f32[2]{0:T(128)S(1)} %slice.28), channel_id=1, source_target_pairs={{0,8},{8,16},{16,24},{1,9},{9,17},{17,25},{2,10},{10,18},{18,26},{... | collective-permute-start | bytes 32 | tf_op jit(solution)/shard_map/ppermute | solution.py:12
  12.3 1.1 convert_multiply_fusion.2
  13.4 3.4 %collective-permute-start.1 = (f32[2,256]{1,0:T(2,128)S(1)}, f32[2,256]{1,0:T(2,128)S(1)}, u32[]{:S(2)}, u32[]{:S(2)}) collective-permute-start(f32[2,256]{1,0:T(2,128)S(1)} %slice.40), channel_id=1, source_target_pairs={{0,8},{8,16},{16,24},{1,9},{9,17},{17,25},{2,10},{10,18},{18,26},{... | collective-permute-start | bytes 6152 | tf_op jit(solution)/shard_map/ppermute | solution.py:12
  16.8 0.8 fusion.42
  17.7 0.8 fusion.35
  18.5 3.6 %convolution_convert_fusion.1 = bf16[512,2048]{1,0:T(8,128)(2,1)} fusion(bf16[256,2048]{1,0:T(8,128)(2,1)} %param.18, f32[2,256]{1,0:T(2,128)S(1)} %collective-permute-done.1, f32[512,256]{1,0:T(8,128)S(1)} %convert_multiply_fusion.2, bf16[512,256]{1,0:T(8,128)(2,1)} %param.13, f32[256]{0:T(256)S(1)} %bitcast.34, f32[256]{0:T(256)S(1)} %bitcast.33, ...), kind=kOutput, calls=%fused_computation.4 | convolution fusion | flops 539492352 | bytes 3938304 | tf_op jit(solution)/shard_map/dot_general | solution.py:59
  22.5 0.2 reduce_window_sum.11
  22.6 0.2 select_reduce_fusion
  22.8 0.1 reduce_sum.44
  23.2 36.8 %reduce-scatter.3.cloned.1.call-done = bf16[64,2048]{1,0:T(8,128)(2,1)} async-done(((bf16[512,2048]{1,0:T(8,128)(2,1)}), bf16[64,2048]{1,0:T(8,128)(2,1)}) %reduce-scatter.3.cloned.1.call-update) | async-done | bytes 262160 | tf_op jit(solution)/shard_map/reduce_scatter | solution.py:58
  59.9 1.1 fusion.14
  61.1 1.4 convolution_convert_fusion.2
  62.5 12.3 %all_to_all.24 = bf16[4,48,2048]{2,1,0:T(8,128)(2,1)} all-to-all(bf16[4,48,2048]{2,1,0:T(8,128)(2,1)S(1)} %bitcast.30), channel_id=1, replica_groups=mesh['sp'=4,'tp'=8] {'sp'}, dimensions={0} | all-to-all | bytes 1572864 | tf_op jit(solution)/shard_map/all_to_all | solution.py:81
  74.8 64.3 %all-gather.2.cloned.1.call-done = bf16[1536,2048]{1,0:T(8,128)(2,1)} async-done(((bf16[192,2048]{1,0:T(8,128)(2,1)}), bf16[1536,2048]{1,0:T(8,128)(2,1)}) %all-gather.2.cloned.1.call-update) | async-done | bytes 6291472 | tf_op jit(solution)/shard_map/all_gather | solution.py:82
  139.1 8.5 %fusion.3 = f32[1536,512]{1,0:T(8,128)} fusion(bf16[1536,2048]{1,0:T(8,128)(2,1)} %all-gather.2.cloned.1.call-done, bf16[1,2048,512]{2,1,0:T(8,128)(2,1)} %param.23), kind=kOutput, calls=%fused_computation.8 | convolution fusion | flops 3221225472 | bytes 11534336 | tf_op jit(solution)/shard_map/dot_general | solution.py:83
  147.6 11.7 %convolution_convert_fusion = bf16[1536,2048]{1,0:T(8,128)(2,1)} fusion(bf16[1,512,2048]{2,1,0:T(8,128)(2,1)S(1)} %copy-done, bf16[1536,2048]{1,0:T(8,128)(2,1)} %all-gather.2.cloned.1.call-done, f32[1536,512]{1,0:T(8,128)} %fusion.3, bf16[1,2048,512]{2,1,0:T(8,128)(2,1)} %param.24), kind=kOutput, calls=%fused_computation.1 | convolution fusion | flops 6450315264 | bytes 19922944 | tf_op jit(solution)/shard_map/dot_general | solution.py:87
  159.4 68.5 %reduce-scatter.5.cloned.1.call-done = bf16[192,2048]{1,0:T(8,128)(2,1)} async-done(((bf16[1536,2048]{1,0:T(8,128)(2,1)}), bf16[192,2048]{1,0:T(8,128)(2,1)}) %reduce-scatter.5.cloned.1.call-update) | async-done | bytes 786448 | tf_op jit(solution)/shard_map/reduce_scatter | solution.py:86
  227.9 3.6 %all-to-all-start.1 = ((bf16[4,48,2048]{2,1,0:T(8,128)(2,1)}), bf16[4,48,2048]{2,1,0:T(8,128)(2,1)S(1)}, u32[]{:S(2)}, u32[]{:S(2)}) async-start(bf16[4,48,2048]{2,1,0:T(8,128)(2,1)} %bitcast.31), calls=%async_computation.3 | async-start | bytes 1572864 | tf_op jit(solution)/shard_map/all_to_all | solution.py:92
  231.8 8.8 %all-to-all-done.1 = bf16[4,48,2048]{2,1,0:T(8,128)(2,1)S(1)} async-done(((bf16[4,48,2048]{2,1,0:T(8,128)(2,1)}), bf16[4,48,2048]{2,1,0:T(8,128)(2,1)S(1)}, u32[]{:S(2)}, u32[]{:S(2)}) %all-to-all-start.1) | async-done | bytes 786464 | tf_op jit(solution)/shard_map/all_to_all | solution.py:92
  240.6 1.7 gather_fusion
  242.3 1.7 reshape.56
  244.0 1.6 multiply_reduce_fusion
  245.6 1.8 fusion.17
  (33 shorter events, 1.1 us)
Async XLA Ops:
  6.5 141.1 %copy-start = (bf16[1,512,2048]{2,1,0:T(8,128)(2,1)S(1)}, bf16[1,512,2048]{2,1,0:T(8,128)(2,1)}, u32[]{:S(2)}) copy-start(bf16[1,512,2048]{2,1,0:T(8,128)(2,1)} %param.25) | copy-start | bytes 6291460
  6.5 53.4 %reduce-scatter.3.cloned.1.call-start = ((), (), s32[]{:S(2)}) async-start(), calls=%async_computation.4 | async-start | bytes 2359296 | tf_op jit(solution)/shard_map/reduce_scatter | solution.py:58
  7.4 10.2 %collective-permute-start = (f32[2]{0:T(128)S(1)}, f32[2]{0:T(128)S(1)}, u32[]{:S(2)}, u32[]{:S(2)}) collective-permute-start(f32[2]{0:T(128)S(1)} %slice.28), channel_id=1, source_target_pairs={{0,8},{8,16},{16,24},{1,9},{9,17},{17,25},{2,10},{10,18},{18,26},{... | collective-permute-start | bytes 32 | tf_op jit(solution)/shard_map/ppermute | solution.py:12
  13.4 5.1 %collective-permute-start.1 = (f32[2,256]{1,0:T(2,128)S(1)}, f32[2,256]{1,0:T(2,128)S(1)}, u32[]{:S(2)}, u32[]{:S(2)}) collective-permute-start(f32[2,256]{1,0:T(2,128)S(1)} %slice.40), channel_id=1, source_target_pairs={{0,8},{8,16},{16,24},{1,9},{9,17},{17,25},{2,10},{10,18},{18,26},{... | collective-permute-start | bytes 6152 | tf_op jit(solution)/shard_map/ppermute | solution.py:12
  18.5 3.7 %copy-start.3 = (s32[64,2]{0,1:T(2,128)S(1)}, s32[64,2]{0,1:T(2,128)}, u32[]{:S(2)}) copy-start(s32[64,2]{0,1:T(2,128)} %param.21) | copy-start | bytes 1540
  18.5 4.6 %copy-start.2 = (bf16[2048]{0:T(1024)(128)(2,1)S(1)}, bf16[2048]{0:T(1024)(128)(2,1)}, u32[]{:S(2)}) copy-start(bf16[2048]{0:T(1024)(128)(2,1)} %param.20) | copy-start | bytes 12292
  18.5 41.5 %copy-start.1 = (bf16[64,2048]{1,0:T(8,128)(2,1)S(1)}, bf16[64,2048]{1,0:T(8,128)(2,1)}, u32[]{:S(2)}) copy-start(bf16[64,2048]{1,0:T(8,128)(2,1)} %param.19) | copy-start | bytes 786436
  22.1 117.0 %all-gather.2.cloned.1.call-start = ((), (), s32[]{:S(2)}) async-start(), calls=%async_computation.5 | async-start | bytes 7077888 | tf_op jit(solution)/shard_map/all_gather | solution.py:82
  74.8 153.1 %reduce-scatter.5.cloned.1.call-start = ((), (), s32[]{:S(2)}) async-start(), calls=%async_computation.6 | async-start | bytes 7077888 | tf_op jit(solution)/shard_map/reduce_scatter | solution.py:86
  159.3 72.3 %copy-start.4 = (f32[64,2]{0,1:T(2,128)S(1)}, f32[64,2]{0,1:T(2,128)}, u32[]{:S(2)}) copy-start(f32[64,2]{0,1:T(2,128)} %param.22) | copy-start | bytes 1540
  227.9 12.7 %all-to-all-start.1 = ((bf16[4,48,2048]{2,1,0:T(8,128)(2,1)}), bf16[4,48,2048]{2,1,0:T(8,128)(2,1)S(1)}, u32[]{:S(2)}, u32[]{:S(2)}) async-start(bf16[4,48,2048]{2,1,0:T(8,128)(2,1)} %bitcast.31), calls=%async_computation.3 | async-start | bytes 1572864 | tf_op jit(solution)/shard_map/all_to_all | solution.py:92
Sparse Core Ops, SparseCore 0:
  22.2 37.6 reduce-scatter.2
  74.9 64.1 all-gather.1
  159.5 68.3 reduce-scatter.4
where the time goes:
time: 254 us
  waiting for transfers between devices  178 us (70%)
  matrix products  25.2 us (10%)
  between operations  13.3 us (5%)
  blocking collectives  12.3 us (5%)
  starting transfers between devices  12 us (5%)
  other arithmetic  7.76 us (3%)
  local copies, waits for them, and re-layouts  4.98 us (2%)
    reduce_scatter x1, waiting for transfers between devices, shards(): lax.psum_scatter(jnp.dot(act, down_weight[0], preferred_element_type=jnp....  68.5 us
    all_gather x1, waiting for transfers between devices, shards(): gathered = lax.all_gather(arrived, 'tp', axis=0, tiled=True)  64.3 us
    reduce_scatter x1, waiting for transfers between devices, shards(): lax.psum_scatter(jnp.dot(gated, out_weight, preferred_element_type=jnp.fl...  36.8 us
    all_to_all x1, blocking collectives, shards(): lax.all_to_all(outgoing, 'sp', split_axis=0, concat_axis=0, tiled=True)  12.3 us
    dot_general x1, matrix products, shards(): jnp.dot(act, down_weight[0], preferred_element_type=jnp.float32)  11.7 us
    all_to_all x1, waiting for transfers between devices, shards(): lax.all_to_all(summed, 'sp', split_axis=0, concat_axis=0, tiled=True)  8.83 us
    dot_general x1, matrix products, shards(): jnp.dot(gathered, gate_weight[0], preferred_element_type=jnp.float32)  8.53 us
    ppermute x2, starting transfers between devices, passed_along(): return lax.ppermute(block, axis, route)  8.26 us
  transfers between devices with their start and end apart: 6, of which 4 were waited for; matrix products, arithmetic and copies ran while one was open for 2% of the time, Pallas kernels for 0%

commit v1 on v0

v1 whole, which is shorter than its diff:
```python
import functools

import jax
import jax.numpy as jnp
from jax import lax
from jax.experimental import pallas as pl
from jax.experimental.pallas import tpu as pltpu
from jax.sharding import PartitionSpec as P

EPS = 1e-06


def passed_along(block, axis, distance):
    devices = range(lax.axis_size(axis))
    route = [(i - distance, i) for i in devices if i - distance in devices]
    return lax.ppermute(block, axis, route)


MESH = pl.DeviceIdType.MESH
CHUNK = 16
COLS = 512


def where_am_i(n_sp, nz):
    s, t = lax.axis_index("sp"), lax.axis_index("tp")
    z, c = t // 2, t % 2
    return s, z, c


def greet(s, z, c, n_sp, nz):
    barrier = pltpu.get_barrier_semaphore()
    peers = [(s, 2 * z + 1 - c)]
    peers += [(s, 2 * lax.rem(z + i, nz) + c) for i in range(1, nz)]
    peers += [(lax.rem(s + k, n_sp), 2 * z + c) for k in range(1, n_sp)]
    for peer in peers:
        pl.semaphore_signal(barrier, inc=1, device_id=peer, device_id_type=MESH)
    pl.semaphore_wait(barrier, len(peers))


def send(src, dst, send_sem, recv_sem, peer):
    copy = pltpu.make_async_remote_copy(
        src_ref=src,
        dst_ref=dst,
        send_sem=send_sem,
        recv_sem=recv_sem,
        device_id=peer,
        device_id_type=MESH,
    )
    copy.start()
    return copy


def by_rows(rows, body):
    def step(r, carry):
        body(pl.ds(pl.multiple_of(r * CHUNK, CHUNK), CHUNK))
        return carry

    lax.fori_loop(0, rows // CHUNK, step, 0)


def by_columns(width, body):
    def step(r, carry):
        body(pl.ds(pl.multiple_of(r * COLS, COLS), COLS))
        return carry

    lax.fori_loop(0, width // COLS, step, 0)


def slot_hits(meta, s, n_sp, cap):
    rows = meta.shape[1]
    slots = lax.broadcasted_iota(jnp.int32, (n_sp * cap, rows), 0).astype(jnp.float32)
    own = s.astype(jnp.float32)
    hits = []
    for k in range(2):
        ahead = meta[2 * k : 2 * k + 1, :] - own
        ahead = jnp.where(ahead < 0.0, ahead + float(n_sp), ahead)
        hits.append(slots == ahead * float(cap) + meta[2 * k + 1 : 2 * k + 2, :])
    return hits


def dispatch_kernel(
    n_sp, nz, cap, part, residual, gain, meta, hidden, metas, gathered,
    rx, stage, rz, nbuf, routed,
    d_send, d_recv, m_send, m_recv, z_send, z_recv, n_send, n_recv, p_send, p_recv, f_send, f_recv,
):
    s, z, c = where_am_i(n_sp, nz)
    o = 1 - c
    partner = (s, 2 * z + o)
    rows, width = residual.shape
    order = list(range(1, nz)) + [0]
    ahead = [lax.rem(z + i, nz) for i in range(nz)]
    greet(s, z, c, n_sp, nz)

    halves = {}
    for i in order:
        halves[i] = send(part.at[ahead[i], o], rx.at[i], d_send.at[i], d_recv.at[i], partner)
    notes = [send(meta, metas.at[i], m_send.at[i], m_recv.at[i], (s, 2 * ahead[i] + c)) for i in range(1, nz)]
    metas[0] = meta[...]

    sums = []
    for i in order:
        halves[i].wait_recv()
        if i:

            def add(r, i=i):
                stage[i, r, :] = (
                    part[ahead[i], c, r, :].astype(jnp.float32) + rx[i, r, :].astype(jnp.float32)
                ).astype(jnp.bfloat16)

            by_rows(rows, add)
            sums.append(send(stage.at[i], rz.at[i], z_send.at[i], z_recv.at[i], (s, 2 * ahead[i] + c)))
    for copy in sums:
        copy.wait_recv()

    def norm(r):
        total = part[z, c, r, :].astype(jnp.float32) + rx[0, r, :].astype(jnp.float32)
        for i in range(1, nz):
            total = total + rz[i, r, :].astype(jnp.float32)
        state = (residual[r, :].astype(jnp.float32) + total).astype(jnp.bfloat16)
        hidden[r, :] = state
        wide = state.astype(jnp.float32)
        stats = jnp.mean(wide * wide, axis=-1, keepdims=True)
        nbuf[0, r, :] = (wide * lax.rsqrt(stats + EPS) * gain[...].astype(jnp.float32)).astype(jnp.bfloat16)

    by_rows(rows, norm)
    spread = [
        send(nbuf.at[0], nbuf.at[i], n_send.at[i], n_recv.at[i], (s, 2 * ahead[i] + c)) for i in range(1, nz)
    ]

    sent, forwards = [], []

    def forward(i):
        for copy in sent[i]:
            copy.wait_recv()
        forwards.append(send(gathered.at[i, 0], gathered.at[i, 1], f_send.at[i], f_recv.at[i], partner))

    for i in range(nz):
        if i:
            notes[i - 1].wait_recv()
            spread[i - 1].wait_recv()
        first, second = slot_hits(metas[i], s, n_sp, cap)
        table = (first | second).astype(jnp.float32).astype(jnp.bfloat16)

        def place(cols, i=i, table=table):
            placed = jnp.dot(table, nbuf[i, :, cols], preferred_element_type=jnp.float32).astype(jnp.bfloat16)
            gathered[i, 0, 0, :, cols] = placed[:cap]
            for k in range(1, n_sp):
                routed[i, k, :, cols] = placed[k * cap : (k + 1) * cap]

        by_columns(width, place)
        sent.append([
            send(
                routed.at[i, k], gathered.at[i, 0, k], p_send.at[i, k], p_recv.at[i, k],
                (lax.rem(s + k, n_sp), 2 * z + c),
            )
            for k in range(1, n_sp)
        ])
        if i:
            forward(i - 1)
    forward(nz - 1)
    for copy in forwards:
        copy.wait_recv()
    for copy in list(halves.values()) + notes + sums + spread + sum(sent, []) + forwards:
        copy.wait_send()


def return_kernel(
    n_sp, nz, cap, partial, hidden, metas, out,
    rx, stage, arrived, mine, combined, zrx,
    d_send, d_recv, p_send, p_recv, z_send, z_recv,
):
    s, z, c = where_am_i(n_sp, nz)
    partner = (s, 2 * z + 1 - c)
    rows, width = hidden.shape
    order = list(range(1, nz)) + [0]
    greet(s, z, c, n_sp, nz)
    halves = {i: send(partial.at[i, 1], rx.at[i], d_send.at[i], d_recv.at[i], partner) for i in order}
    sent = {}
    for i in order:
        halves[i].wait_recv()

        def add(cols, i=i):
            total = partial[i, 0, :, :, cols].astype(jnp.float32) + rx[i, :, :, cols].astype(jnp.float32)
            total = total.astype(jnp.bfloat16)
            stage[i, :, :, cols] = total

        by_columns(width, add)
        sent[i] = [
            send(
                stage.at[i, k], arrived.at[i, k], p_send.at[i, k], p_recv.at[i, k],
                (lax.rem(s + n_sp - k, n_sp), 2 * z + c),
            )
            for k in range(1, n_sp)
        ]
    back = []
    for i in order:
        for copy in sent[i]:
            copy.wait_recv()
        meta = metas[i]
        first, second = slot_hits(meta, s, n_sp, cap)
        weights = jnp.where(first, meta[4:5, :], 0.0) + jnp.where(second, meta[5:6, :], 0.0)
        high = weights.astype(jnp.bfloat16)
        low = (weights - high.astype(jnp.float32)).astype(jnp.bfloat16)

        def combine(cols, i=i, high=high, low=low):
            own = stage[i, 0, :, cols]
            others = [arrived[i, k, :, cols] for k in range(1, n_sp)]
            values = jnp.concatenate([own] + others, axis=0)
            dims = (((0,), (0,)), ((), ()))
            total = lax.dot_general(high, values, dims, preferred_element_type=jnp.float32)
            total = total + lax.dot_general(low, values, dims, preferred_element_type=jnp.float32)
            if i:
                combined[i, :, cols] = total.astype(jnp.bfloat16)
            else:
                mine[:, cols] = total

        by_columns(width, combine)
        if i:
            back.append(
                send(
                    combined.at[i], zrx.at[i], z_send.at[i], z_recv.at[i],
                    (s, 2 * lax.rem(z + nz - i, nz) + c),
                )
            )
    for copy in back:
        copy.wait_recv()

    def finish(r):
        total = mine[r, :]
        for i in range(1, nz):
            total = total + zrx[i, r, :].astype(jnp.float32)
        out[r, :] = (hidden[r, :].astype(jnp.float32) + total).astype(jnp.bfloat16)

    by_rows(rows, finish)
    for copy in list(halves.values()) + sum(sent.values(), []) + back:
        copy.wait_send()


VMEM_LIMIT = 60 * 1024 * 1024


def dispatch(part, residual, gain, meta, n_sp, nz, cap):
    rows, width = residual.shape
    bf16, dma = jnp.bfloat16, pltpu.SemaphoreType.DMA
    vmem = pl.BlockSpec(memory_space=pltpu.VMEM)
    return pl.pallas_call(
        functools.partial(dispatch_kernel, n_sp, nz, cap),
        out_shape=(
            jax.ShapeDtypeStruct((rows, width), bf16),
            jax.ShapeDtypeStruct((nz,) + meta.shape, jnp.float32),
            jax.ShapeDtypeStruct((nz, 2, n_sp, cap, width), bf16),
        ),
        in_specs=[vmem] * 4,
        out_specs=(vmem,) * 3,
        scratch_shapes=[
            pltpu.VMEM((nz, rows, width), bf16),
            pltpu.VMEM((nz, rows, width), bf16),
            pltpu.VMEM((nz, rows, width), bf16),
            pltpu.VMEM((nz, rows, width), bf16),
            pltpu.VMEM((nz, n_sp, cap, width), bf16),
        ]
        + [dma((nz,))] * 8
        + [dma((nz, n_sp))] * 2
        + [dma((nz,))] * 2,
        compiler_params=pltpu.CompilerParams(
            collective_id=0, has_side_effects=True, vmem_limit_bytes=VMEM_LIMIT
        ),
    )(part, residual, gain, meta)


def give_back(partial, hidden, metas, n_sp, nz, cap):
    rows, width = hidden.shape
    bf16, dma = jnp.bfloat16, pltpu.SemaphoreType.DMA
    vmem = pl.BlockSpec(memory_space=pltpu.VMEM)
    return pl.pallas_call(
        functools.partial(return_kernel, n_sp, nz, cap),
        out_shape=jax.ShapeDtypeStruct((rows, width), bf16),
        in_specs=[vmem] * 3,
        out_specs=vmem,
        scratch_shapes=[
            pltpu.VMEM((nz, n_sp, cap, width), bf16),
            pltpu.VMEM((nz, n_sp, cap, width), bf16),
            pltpu.VMEM((nz, n_sp, cap, width), bf16),
            pltpu.VMEM((rows, width), jnp.float32),
            pltpu.VMEM((nz, rows, width), bf16),
            pltpu.VMEM((nz, rows, width), bf16),
        ]
        + [dma((nz,))] * 2
        + [dma((nz, n_sp))] * 2
        + [dma((nz,))] * 2,
        compiler_params=pltpu.CompilerParams(
            collective_id=1, has_side_effects=True, vmem_limit_bytes=VMEM_LIMIT
        ),
    )(partial, hidden, metas)


def describe(expert_ids, route_weights, experts):
    onehot = (expert_ids[:, :, None] == jnp.arange(experts, dtype=jnp.int32)).astype(jnp.float32)
    named = jnp.sum(onehot, axis=1)
    count = named.shape[0]
    before = jnp.arange(count)[:, None] > jnp.arange(count)[None, :]
    earlier = jnp.sum(jnp.where(before[:, :, None], named[None, :, :], 0.0), axis=1)
    slot = jnp.sum(earlier[:, None, :] * onehot, axis=2)
    ids = expert_ids.astype(jnp.float32)
    zero = jnp.zeros_like(slot[:, 0])
    return jnp.stack(
        [ids[:, 0], slot[:, 0], ids[:, 1], slot[:, 1], route_weights[:, 0], route_weights[:, 1], zero, zero]
    )


def shards(
    out_gate,
    in_gate,
    conv_input,
    conv_taps,
    documents,
    out_weight,
    residual,
    norm_gain,
    expert_ids,
    route_weights,
    gate_weight,
    up_weight,
    down_weight,
):
    length = conv_input.shape[0]
    signal = in_gate.astype(jnp.float32) * conv_input.astype(jnp.float32)
    doc_values = documents.astype(jnp.float32)
    prior_signal, prior_docs = passed_along(
        (signal[length - 2 :], doc_values[length - 2 :]), "sp", 1
    )
    long_signal = jnp.concatenate([prior_signal, signal], axis=0)
    long_docs = jnp.concatenate([prior_docs, doc_values], axis=0)
    position = lax.axis_index("sp") * length + jnp.arange(length, dtype=jnp.int32)
    tap_values = conv_taps.astype(jnp.float32)
    mixed_conv = tap_values[2][None, :] * signal
    for offset in (1, 2):
        earlier_signal = long_signal[2 - offset : 2 - offset + length]
        earlier_docs = long_docs[2 - offset : 2 - offset + length]
        allowed = (position >= offset) & (earlier_docs == doc_values)
        mixed_conv = mixed_conv + jnp.where(
            allowed[:, None], tap_values[2 - offset][None, :] * earlier_signal, 0.0
        )
    gated = (out_gate.astype(jnp.float32) * mixed_conv).astype(jnp.bfloat16)
    block_rows = length // lax.axis_size("tp")
    n_sp, nz = lax.axis_size("sp"), lax.axis_size("tp") // 2
    width = residual.shape[1]
    capacity = max(2, (3 * block_rows + n_sp - 1) // n_sp)
    cap = -(-capacity // CHUNK) * CHUNK
    meta = describe(expert_ids, route_weights, n_sp)
    part = jnp.dot(gated, out_weight, preferred_element_type=jnp.float32).astype(jnp.bfloat16)
    hidden, metas, gathered = dispatch(
        part.reshape(nz, 2, block_rows, width), residual, norm_gain[None, :], meta, n_sp, nz, cap
    )
    rows = gathered.reshape(-1, width)
    gate_proj = jnp.dot(rows, gate_weight[0], preferred_element_type=jnp.float32)
    up_proj = jnp.dot(rows, up_weight[0], preferred_element_type=jnp.float32)
    act = (jax.nn.silu(gate_proj) * up_proj).astype(jnp.bfloat16)
    partial = jnp.dot(act, down_weight[0], preferred_element_type=jnp.float32).astype(jnp.bfloat16)
    return give_back(partial.reshape(gathered.shape), hidden, metas, n_sp, nz, cap)


def solution(mesh):
    in_specs = (
        P("sp", "tp"),
        P("sp", "tp"),
        P("sp", "tp"),
        P(None, "tp"),
        P("sp"),
        P("tp", None),
        P(("sp", "tp"), None),
        P(),
        P(("sp", "tp"), None),
        P(("sp", "tp"), None),
        P("sp", None, "tp"),
        P("sp", None, "tp"),
        P("sp", "tp", None),
    )
    out_specs = P(("sp", "tp"), None)
    return jax.shard_map(shards, mesh=mesh, in_specs=in_specs, out_specs=out_specs, check_vma=False)
```

time: 254 us -> 173 us (0.68)
  waiting for transfers between devices: 178 us -> 0.01 us
  Pallas kernels: 0 us -> 130 us
  between operations: 13.3 us -> 0.08 us
  blocking collectives: 12.3 us -> 0 us
  starting transfers between devices: 12 us -> 8.26 us
  other arithmetic: 7.76 us -> 4.95 us
    pallas_call x0 -> x2, Pallas kernels: none -> 130 us  [the longest x1 73.4 us: dispatch(): pl.pallas_call(functools.partial(dispatch_kernel, n_sp, nz, cap), out_sha...]
    reduce_scatter x2 -> x0, waiting for transfers between devices: 105 us -> none  [the longest x1 68.5 us: shards(): lax.psum_scatter(jnp.dot(act, down_weight[0], preferred_element_type=jnp....]
    all_gather x1 -> x0, waiting for transfers between devices: 64.3 us -> none  [shards(): gathered = lax.all_gather(arrived, 'tp', axis=0, tiled=True)]
    all_to_all x1 -> x0, blocking collectives: 12.3 us -> none  [shards(): lax.all_to_all(outgoing, 'sp', split_axis=0, concat_axis=0, tiled=True)]
    all_to_all x1 -> x0, waiting for transfers between devices: 8.83 us -> none  [shards(): lax.all_to_all(summed, 'sp', split_axis=0, concat_axis=0, tiled=True)]
    all_to_all x1 -> x0, starting transfers between devices: 3.63 us -> none  [shards(): lax.all_to_all(summed, 'sp', split_axis=0, concat_axis=0, tiled=True)]
    dot_general x2 -> x1, matrix products: 9.91 us -> 8.52 us  [shards(): jnp.dot(rows, gate_weight[0], preferred_element_type=jnp.float32)]
  transfers between devices with their start and end apart: 6 -> 2, of which waited for: 4 -> 0; matrix products, arithmetic and copies ran while one was open for 2% -> 4% of each run, Pallas kernels for 0% -> 0%
where the time goes in v1:
time: 173 us
  Pallas kernels  130 us (75%)
  matrix products  23.8 us (14%)
  starting transfers between devices  8.26 us (5%)
  local copies, waits for them, and re-layouts  5.21 us (3%)
  other arithmetic  4.95 us (3%)
    pallas_call x1, Pallas kernels, dispatch(): pl.pallas_call(functools.partial(dispatch_kernel, n_sp, nz, cap), out_sha...  73.4 us
    pallas_call x1, Pallas kernels, give_back(): pl.pallas_call(functools.partial(return_kernel, n_sp, nz, cap), out_shape...  57 us
    dot_general x1, matrix products, shards(): jnp.dot(act, down_weight[0], preferred_element_type=jnp.float32)  11.7 us
    dot_general x1, matrix products, shards(): jnp.dot(rows, gate_weight[0], preferred_element_type=jnp.float32)  8.52 us
    ppermute x2, starting transfers between devices, passed_along(): return lax.ppermute(block, axis, route)  8.26 us
    dot_general x1, matrix products, shards(): jnp.dot(gated, out_weight, preferred_element_type=jnp.float32)  3.53 us
  transfers between devices with their start and end apart: 2, of which 0 were waited for; matrix products, arithmetic and copies ran while one was open for 4% of the time, Pallas kernels for 0%

profile of v1, /device:TPU:0, one launch (start us, length us, event | category | flops | bytes accessed | tf_op | source)
XLA Modules:
  0.0 172.7 jit_solution(15243251778146430595)
XLA Ops:
  0.0 0.0 copy-start
  0.0 0.8 convert_element_type.37
  0.8 0.1 slice.46
  0.9 4.9 %collective-permute-start = (f32[2]{0:T(128)S(1)}, f32[2]{0:T(128)S(1)}, u32[]{:S(2)}, u32[]{:S(2)}) collective-permute-start(f32[2]{0:T(128)S(1)} %slice.46), channel_id=1, source_target_pairs={{0,8},{8,16},{16,24},{1,9},{9,17},{17,25},{2,10},{10,18},{18,26},{... | collective-permute-start | bytes 32 | tf_op jit(solution)/shard_map/ppermute | solution.py:16
  5.8 1.1 convert_multiply_fusion
  6.9 3.4 %collective-permute-start.1 = (f32[2,256]{1,0:T(2,128)S(1)}, f32[2,256]{1,0:T(2,128)S(1)}, u32[]{:S(2)}, u32[]{:S(2)}) collective-permute-start(f32[2,256]{1,0:T(2,128)S(1)} %slice.62), channel_id=1, source_target_pairs={{0,8},{8,16},{16,24},{1,9},{9,17},{17,25},{2,10},{10,18},{18,26},{... | collective-permute-start | bytes 6152 | tf_op jit(solution)/shard_map/ppermute | solution.py:16
  10.3 0.7 convert_element_type.40
  11.0 0.7 convert_reduce_fusion
  11.7 0.8 fusion.30
  12.5 1.3 broadcast_in_dim.53.gain
  13.8 0.1 select_reduce_fusion
  13.9 0.7 select_reduce_fusion.1
  14.6 0.8 slice_bitcast_fusion
  15.4 0.6 stack.7.meta
  16.0 0.0 collective-permute-done
  16.0 0.1 pad_maximum_fusion.1
  16.0 0.8 fusion.25
  16.8 0.0 collective-permute-done.1
  16.8 3.5 %convolution_convert_fusion.1 = bf16[512,2048]{1,0:T(8,128)(2,1)} fusion(bf16[256,2048]{1,0:T(8,128)(2,1)} %param.18, f32[2,256]{1,0:T(2,128)S(1)} %collective-permute-done.1, f32[512,256]{1,0:T(8,128)S(1)} %convert_multiply_fusion, bf16[512,256]{1,0:T(8,128)(2,1)} %param.13, f32[256]{0:T(256)S(1)} %bitcast.36, f32[256]{0:T(256)S(1)} %bitcast.35, ...), kind=kOutput, calls=%fused_computation.3 | convolution fusion | flops 539492352 | bytes 3938304 | tf_op jit(solution)/shard_map/dot_general | solution.py:351
  20.3 73.4 %shard_map.127 = (bf16[64,2048]{1,0:T(8,128)(2,1)}, f32[4,8,64]{2,1,0:T(8,128)}, bf16[4,2,4,48,2048]{4,3,2,1,0:T(8,128)(2,1)}) custom-call(bf16[4,2,64,2048]{3,2,1,0:T(8,128)(2,1)} %bitcast.33, bf16[64,2048]{1,0:T(8,128)(2,1)} %residual.1, bf16[1,2048]{1,0:T(2,128)(2,1)} %broadcast_in_dim.53.gain, f32[8,64]{1,0:T(8,128)} %stack.7.meta), custom_call_target="tpu_custom_call" | custom-call | tf_op jit(solution)/shard_map/pallas_call | solution.py:246
  93.8 8.5 %fusion.3 = f32[1536,512]{1,0:T(8,128)} fusion(bf16[1536,2048]{1,0:T(8,128)(2,1)} %bitcast.37, bf16[1,2048,512]{2,1,0:T(8,128)(2,1)} %param.23), kind=kOutput, calls=%fused_computation.6 | convolution fusion | flops 3221225472 | bytes 11534336 | tf_op jit(solution)/shard_map/dot_general | solution.py:356
  102.3 11.7 %convolution_convert_fusion = bf16[1536,2048]{1,0:T(8,128)(2,1)} fusion(bf16[1,512,2048]{2,1,0:T(8,128)(2,1)S(1)} %copy-done, bf16[1536,2048]{1,0:T(8,128)(2,1)} %bitcast.38, f32[1536,512]{1,0:T(8,128)} %fusion.3, bf16[1,2048,512]{2,1,0:T(8,128)(2,1)} %param.24), kind=kOutput, calls=%fused_computation | convolution fusion | flops 6450315264 | bytes 19922944 | tf_op jit(solution)/shard_map/dot_general | solution.py:359
  114.1 57.0 %shard_map.128 = bf16[64,2048]{1,0:T(8,128)(2,1)} custom-call(bf16[4,2,4,48,2048]{4,3,2,1,0:T(8,128)(2,1)} %bitcast.32, bf16[64,2048]{1,0:T(8,128)(2,1)} %get-tuple-element.9.hidden, f32[4,8,64]{2,1,0:T(8,128)} %get-tuple-element.10.metas), custom_call_target="tpu_custom_call" | custom-call | tf_op jit(solution)/shard_map/pallas_call | solution.py:275
  171.1 1.7 copy.16
  (5 shorter events, 0.0 us)
Async XLA Ops:
  0.0 102.3 %copy-start = (bf16[1,512,2048]{2,1,0:T(8,128)(2,1)S(1)}, bf16[1,512,2048]{2,1,0:T(8,128)(2,1)}, u32[]{:S(2)}) copy-start(bf16[1,512,2048]{2,1,0:T(8,128)(2,1)} %param.25) | copy-start | bytes 6291460
  0.9 15.1 %collective-permute-start = (f32[2]{0:T(128)S(1)}, f32[2]{0:T(128)S(1)}, u32[]{:S(2)}, u32[]{:S(2)}) collective-permute-start(f32[2]{0:T(128)S(1)} %slice.46), channel_id=1, source_target_pairs={{0,8},{8,16},{16,24},{1,9},{9,17},{17,25},{2,10},{10,18},{18,26},{... | collective-permute-start | bytes 32 | tf_op jit(solution)/shard_map/ppermute | solution.py:16
  6.9 9.9 %collective-permute-start.1 = (f32[2,256]{1,0:T(2,128)S(1)}, f32[2,256]{1,0:T(2,128)S(1)}, u32[]{:S(2)}, u32[]{:S(2)}) collective-permute-start(f32[2,256]{1,0:T(2,128)S(1)} %slice.62), channel_id=1, source_target_pairs={{0,8},{8,16},{16,24},{1,9},{9,17},{17,25},{2,10},{10,18},{18,26},{... | collective-permute-start | bytes 6152 | tf_op jit(solution)/shard_map/ppermute | solution.py:16

commit v2 on v1

v2 whole, which is shorter than its diff:
```python
import functools

import jax
import jax.numpy as jnp
from jax import lax
from jax.experimental import pallas as pl
from jax.experimental.pallas import tpu as pltpu
from jax.sharding import PartitionSpec as P

EPS = 1e-06


MESH = pl.DeviceIdType.MESH
CHUNK = 16
COLS = 512
UNITS = 256
HALO = 8
STRIP = 64
LANES = 128
VMEM_LIMIT = 63 * 1024 * 1024


def where_am_i(n_sp, nz):
    s, t = lax.axis_index("sp"), lax.axis_index("tp")
    z, c = t // 2, t % 2
    return s, z, c


def greet(s, z, c, n_sp, nz):
    barrier = pltpu.get_barrier_semaphore()
    peers = [(s, 2 * z + 1 - c)]
    peers += [(s, 2 * lax.rem(z + i, nz) + c) for i in range(1, nz)]
    peers += [(lax.rem(s + k, n_sp), 2 * z + c) for k in range(1, n_sp)]
    for peer in peers:
        pl.semaphore_signal(barrier, inc=1, device_id=peer, device_id_type=MESH)
    return lambda: pl.semaphore_wait(barrier, len(peers))


def send(src, dst, send_sem, recv_sem, peer):
    copy = pltpu.make_async_remote_copy(
        src_ref=src,
        dst_ref=dst,
        send_sem=send_sem,
        recv_sem=recv_sem,
        device_id=peer,
        device_id_type=MESH,
    )
    copy.start()
    return copy


def by_rows(rows, body):
    def step(r, carry):
        body(pl.ds(pl.multiple_of(r * CHUNK, CHUNK), CHUNK))
        return carry

    lax.fori_loop(0, rows // CHUNK, step, 0)


def by_columns(width, body):
    def step(r, carry):
        body(pl.ds(pl.multiple_of(r * COLS, COLS), COLS))
        return carry

    lax.fori_loop(0, width // COLS, step, 0)


def slot_hits(meta, s, n_sp, cap):
    rows = meta.shape[1]
    slots = lax.broadcasted_iota(jnp.int32, (n_sp * cap, rows), 0).astype(jnp.float32)
    own = s.astype(jnp.float32)
    hits = []
    for k in range(2):
        ahead = meta[2 * k : 2 * k + 1, :] - own
        ahead = jnp.where(ahead < 0.0, ahead + float(n_sp), ahead)
        hits.append(slots == ahead * float(cap) + meta[2 * k + 1 : 2 * k + 2, :])
    return hits


def describe(routes, meta, n_sp):
    rows = routes.shape[1]
    choice = [routes[0:1, :], routes[1:2, :]]
    expert = lax.broadcasted_iota(jnp.int32, (-(-n_sp // CHUNK) * CHUNK, rows), 0).astype(jnp.float32)
    names = [expert == choice[0], expert == choice[1]]
    named = (names[0] | names[1]).astype(jnp.float32).astype(jnp.bfloat16)
    before = lax.broadcasted_iota(jnp.int32, (rows, rows), 0) < lax.broadcasted_iota(jnp.int32, (rows, rows), 1)
    earlier = jnp.dot(
        named, before.astype(jnp.float32).astype(jnp.bfloat16), preferred_element_type=jnp.float32
    )
    for k in range(2):
        meta[2 * k : 2 * k + 1, :] = choice[k]
        meta[2 * k + 1 : 2 * k + 2, :] = jnp.sum(jnp.where(names[k], earlier, 0.0), axis=0, keepdims=True)
    meta[4:6, :] = routes[2:4, :]
    meta[6:8, :] = jnp.zeros((2, rows), jnp.float32)


def layer_kernel(
    n_sp, nz, cap,
    in_gate, conv_input, out_gate, taps, docs, out_weight, residual, gain, routes, gate_hbm, up_hbm, down_hbm,
    out,
    gate, up, down, signal, long_docs, tail_signal, tail_docs, halo_signal, halo_docs, gated, part, meta, metas,
    hidden, rx, stage, rz, nbuf, routed, gathered, act, half_rx, arrived, mine, combined, zrx,
    w_sem, h_send, h_recv,
    d_send, d_recv, m_send, m_recv, z_send, z_recv, n_send, n_recv, p_send, p_recv, f_send, f_recv,
    e_send, e_recv, r_send, r_recv, b_send, b_recv,
):
    s, z, c = where_am_i(n_sp, nz)
    o = 1 - c
    partner = (s, 2 * z + o)
    rows, width = residual.shape
    length, channels = in_gate.shape
    order = list(range(1, nz)) + [0]
    ahead = [lax.rem(z + i, nz) for i in range(nz)]
    greeted = greet(s, z, c, n_sp, nz)
    loads = [
        pltpu.make_async_copy(src, dst, w_sem.at[i])
        for i, (src, dst) in enumerate([(gate_hbm, gate), (up_hbm, up), (down_hbm, down)])
    ]
    for load in loads:
        load.start()

    tail = slice(length - HALO, length)
    tail_signal[...] = in_gate[tail, :].astype(jnp.float32) * conv_input[tail, :].astype(jnp.float32)
    tail_docs[...] = docs[tail, :]
    signal[HALO:, :] = in_gate[...].astype(jnp.float32) * conv_input[...].astype(jnp.float32)
    long_docs[HALO:, :] = docs[...]
    describe(routes, meta, n_sp)
    metas[0] = meta[...]
    greeted()
    following = (lax.rem(s + 1, n_sp), 2 * z + c)
    halo = [
        send(tail_signal, halo_signal, h_send.at[0], h_recv.at[0], following),
        send(tail_docs, halo_docs, h_send.at[1], h_recv.at[1], following),
    ]
    for copy in halo:
        copy.wait_recv()
    signal[:HALO, :] = halo_signal[...]
    long_docs[:HALO, :] = jnp.where(s == 0, -1.0, halo_docs[...])
    tap_values = taps[...].astype(jnp.float32)
    for r in range(0, length, STRIP):
        at = [slice(HALO + r - j, HALO + r - j + STRIP) for j in range(3)]
        here = long_docs[at[0], :]
        same = [None] + [long_docs[at[j], :] == here for j in (1, 2)]
        for l in range(0, channels, LANES):
            lane = slice(l, l + LANES)
            conv = tap_values[2:3, lane] * signal[at[0], lane]
            for j in (1, 2):
                conv = conv + jnp.where(same[j], tap_values[2 - j : 3 - j, lane] * signal[at[j], lane], 0.0)
            gated[r : r + STRIP, lane] = (out_gate[r : r + STRIP, lane].astype(jnp.float32) * conv).astype(
                jnp.bfloat16
            )

    def project(cols):
        part[:, cols] = jnp.dot(
            gated[...], out_weight[:, cols], preferred_element_type=jnp.float32
        ).astype(jnp.bfloat16)

    by_columns(width, project)

    def block(at_z, core):
        return pl.multiple_of((2 * at_z + core) * rows, rows)

    halves = {}
    for i in order:
        halves[i] = send(
            part.at[pl.ds(block(ahead[i], o), rows)], rx.at[i], d_send.at[i], d_recv.at[i], partner
        )
    notes = [send(meta, metas.at[i], m_send.at[i], m_recv.at[i], (s, 2 * ahead[i] + c)) for i in range(1, nz)]
    sums = []
    for i in order:
        halves[i].wait_recv()
        if i:

            def add(r, i=i):
                own = part[pl.ds(pl.multiple_of(block(ahead[i], c) + r.start, CHUNK), CHUNK), :]
                stage[i, r, :] = (own.astype(jnp.float32) + rx[i, r, :].astype(jnp.float32)).astype(jnp.bfloat16)

            by_rows(rows, add)
            sums.append(send(stage.at[i], rz.at[i], z_send.at[i], z_recv.at[i], (s, 2 * ahead[i] + c)))
    for copy in sums:
        copy.wait_recv()

    def norm(r):
        own = part[pl.ds(pl.multiple_of(block(z, c) + r.start, CHUNK), CHUNK), :]
        total = own.astype(jnp.float32) + rx[0, r, :].astype(jnp.float32)
        for i in range(1, nz):
            total = total + rz[i, r, :].astype(jnp.float32)
        state = (residual[r, :].astype(jnp.float32) + total).astype(jnp.bfloat16)
        hidden[r, :] = state
        wide = state.astype(jnp.float32)
        stats = jnp.mean(wide * wide, axis=-1, keepdims=True)
        nbuf[0, r, :] = (wide * lax.rsqrt(stats + EPS) * gain[...].astype(jnp.float32)).astype(jnp.bfloat16)

    by_rows(rows, norm)
    spread = [
        send(nbuf.at[0], nbuf.at[i], n_send.at[i], n_recv.at[i], (s, 2 * ahead[i] + c)) for i in range(1, nz)
    ]

    sent, forwards, swaps, returns, back = {}, {}, {}, {}, []

    def build(i):
        if i:
            notes[i - 1].wait_recv()
            spread[i - 1].wait_recv()
        first, second = slot_hits(metas[i], s, n_sp, cap)
        table = (first | second).astype(jnp.float32).astype(jnp.bfloat16)

        def place(cols):
            placed = jnp.dot(table, nbuf[i, :, cols], preferred_element_type=jnp.float32).astype(jnp.bfloat16)
            gathered[i, 0, 0, :, cols] = placed[:cap]
            for k in range(1, n_sp):
                routed[i, k, :, cols] = placed[k * cap : (k + 1) * cap]

        by_columns(width, place)
        sent[i] = [
            send(
                routed.at[i, k], gathered.at[i, 0, k], p_send.at[i, k], p_recv.at[i, k],
                (lax.rem(s + k, n_sp), 2 * z + c),
            )
            for k in range(1, n_sp)
        ]

    def forward(i):
        for copy in sent[i]:
            copy.wait_recv()
        forwards[i] = send(gathered.at[i, 0], gathered.at[i, 1], f_send.at[i], f_recv.at[i], partner)

    def expert(i):
        if i == 0:
            for load in loads:
                load.wait()
        forwards[i].wait_recv()
        half = n_sp * cap
        hidden_units = gate.shape[1]
        step = min(UNITS, hidden_units)

        def inner(r, carry):
            units = pl.ds(pl.multiple_of(r * step, step), step)
            held = gathered[i].reshape(2 * half, width)
            gate_proj = jnp.dot(held, gate[:, units], preferred_element_type=jnp.float32)
            up_proj = jnp.dot(held, up[:, units], preferred_element_type=jnp.float32)
            act[:, units] = (gate_proj / (1.0 + jnp.exp(-gate_proj)) * up_proj).astype(jnp.bfloat16)
            return carry

        lax.fori_loop(0, hidden_units // step, inner, 0)
        for copy in sent[i]:
            copy.wait_send()
        forwards[i].wait_send()

        def outer(cols):
            share = jnp.dot(act[...], down[:, cols], preferred_element_type=jnp.float32).astype(jnp.bfloat16)
            routed[i, :, :, cols] = share[:half].reshape(n_sp, cap, COLS)
            gathered[i, 0, :, :, cols] = share[half:].reshape(n_sp, cap, COLS)

        by_columns(width, outer)
        swaps[i] = send(gathered.at[i, 0], half_rx.at[i], e_send.at[i], e_recv.at[i], partner)

    def give_back(i):
        swaps[i].wait_recv()

        def add(cols):
            total = routed[i, :, :, cols].astype(jnp.float32) + half_rx[i, :, :, cols].astype(jnp.float32)
            routed[i, :, :, cols] = total.astype(jnp.bfloat16)

        by_columns(width, add)
        returns[i] = [
            send(
                routed.at[i, k], arrived.at[i, k], r_send.at[i, k], r_recv.at[i, k],
                (lax.rem(s + n_sp - k, n_sp), 2 * z + c),
            )
            for k in range(1, n_sp)
        ]

    def combine(i):
        for copy in returns[i]:
            copy.wait_recv()
        weight_rows = metas[i]
        first, second = slot_hits(weight_rows, s, n_sp, cap)
        weights = jnp.where(first, weight_rows[4:5, :], 0.0) + jnp.where(second, weight_rows[5:6, :], 0.0)
        high = weights.astype(jnp.bfloat16)
        low = (weights - high.astype(jnp.float32)).astype(jnp.bfloat16)

        def weigh(cols):
            values = jnp.concatenate(
                [routed[i, 0, :, cols]] + [arrived[i, k, :, cols] for k in range(1, n_sp)], axis=0
            )
            dims = (((0,), (0,)), ((), ()))
            total = lax.dot_general(high, values, dims, preferred_element_type=jnp.float32)
            total = total + lax.dot_general(low, values, dims, preferred_element_type=jnp.float32)
            if i:
                combined[i, :, cols] = total.astype(jnp.bfloat16)
            else:
                mine[:, cols] = total

        by_columns(width, weigh)
        if i:
            back.append(
                send(
                    combined.at[i], zrx.at[i], b_send.at[i], b_recv.at[i], (s, 2 * lax.rem(z + nz - i, nz) + c)
                )
            )

    for i in range(nz):
        build(i)
        if i >= 1:
            forward(i - 1)
        if i >= 2:
            expert(i - 2)
            if i >= 3:
                give_back(i - 2)
    forward(nz - 1)
    for i in range(max(nz - 2, 0), nz):
        expert(i)
        if i:
            give_back(i)
    give_back(0)
    for i in order:
        combine(i)
    for copy in back:
        copy.wait_recv()

    def finish(r):
        total = mine[r, :]
        for i in range(1, nz):
            total = total + zrx[i, r, :].astype(jnp.float32)
        out[r, :] = (hidden[r, :].astype(jnp.float32) + total).astype(jnp.bfloat16)

    by_rows(rows, finish)
    left = halo + list(halves.values()) + notes + sums + spread + list(swaps.values()) + back
    for copy in left + sum(returns.values(), []):
        copy.wait_send()


def shards(
    out_gate,
    in_gate,
    conv_input,
    conv_taps,
    documents,
    out_weight,
    residual,
    norm_gain,
    expert_ids,
    route_weights,
    gate_weight,
    up_weight,
    down_weight,
):
    n_sp, nz = lax.axis_size("sp"), lax.axis_size("tp") // 2
    length, channels = conv_input.shape
    rows, width = residual.shape
    units = gate_weight.shape[2]
    capacity = max(2, (3 * rows + n_sp - 1) // n_sp)
    cap = -(-capacity // CHUNK) * CHUNK
    docs = jnp.broadcast_to(documents.astype(jnp.float32)[:, None], (length, LANES))
    routes = jnp.concatenate([expert_ids.astype(jnp.float32).T, route_weights.T], axis=0)
    bf16, f32, dma = jnp.bfloat16, jnp.float32, pltpu.SemaphoreType.DMA
    vmem, hbm = pl.BlockSpec(memory_space=pltpu.VMEM), pl.BlockSpec(memory_space=pltpu.HBM)
    per_z = pltpu.VMEM((nz, rows, width), bf16)
    slots = pltpu.VMEM((nz, n_sp, cap, width), bf16)
    return pl.pallas_call(
        functools.partial(layer_kernel, n_sp, nz, cap),
        out_shape=jax.ShapeDtypeStruct((rows, width), bf16),
        in_specs=[vmem] * 9 + [hbm] * 3,
        out_specs=vmem,
        scratch_shapes=[
            pltpu.VMEM((width, units), bf16),
            pltpu.VMEM((width, units), bf16),
            pltpu.VMEM((units, width), bf16),
            pltpu.VMEM((HALO + length, channels), f32),
            pltpu.VMEM((HALO + length, LANES), f32),
            pltpu.VMEM((HALO, channels), f32),
            pltpu.VMEM((HALO, LANES), f32),
            pltpu.VMEM((HALO, channels), f32),
            pltpu.VMEM((HALO, LANES), f32),
            pltpu.VMEM((length, channels), bf16),
            pltpu.VMEM((length, width), bf16),
            pltpu.VMEM((8, rows), f32),
            pltpu.VMEM((nz, 8, rows), f32),
            pltpu.VMEM((rows, width), bf16),
            per_z,
            per_z,
            per_z,
            per_z,
            slots,
            pltpu.VMEM((nz, 2, n_sp, cap, width), bf16),
            pltpu.VMEM((2 * n_sp * cap, units), bf16),
            slots,
            slots,
            pltpu.VMEM((rows, width), f32),
            per_z,
            per_z,
            dma((3,)),
            dma((2,)),
            dma((2,)),
        ]
        + [dma((nz,))] * 8
        + [dma((nz, n_sp))] * 2
        + [dma((nz,))] * 4
        + [dma((nz, n_sp))] * 2
        + [dma((nz,))] * 2,
        compiler_params=pltpu.CompilerParams(
            collective_id=0, has_side_effects=True, vmem_limit_bytes=VMEM_LIMIT
        ),
    )(
        in_gate, conv_input, out_gate, conv_taps, docs, out_weight, residual, norm_gain[None, :], routes,
        gate_weight[0], up_weight[0], down_weight[0],
    )


def solution(mesh):
    in_specs = (
        P("sp", "tp"),
        P("sp", "tp"),
        P("sp", "tp"),
        P(None, "tp"),
        P("sp"),
        P("tp", None),
        P(("sp", "tp"), None),
        P(),
        P(("sp", "tp"), None),
        P(("sp", "tp"), None),
        P("sp", None, "tp"),
        P("sp", None, "tp"),
        P("sp", "tp", None),
    )
    out_specs = P(("sp", "tp"), None)
    return jax.shard_map(shards, mesh=mesh, in_specs=in_specs, out_specs=out_specs, check_vma=False)
```

time: 173 us -> 130 us (0.75)
  matrix products: 23.8 us -> 0 us
  starting transfers between devices: 8.26 us -> 0 us
  Pallas kernels: 130 us -> 123 us
  other arithmetic: 4.95 us -> 2.63 us
    dot_general x3 -> x0, matrix products: 23.8 us -> none  [the longest x1 11.7 us: shards(): jnp.dot(act, down_weight[0], preferred_element_type=jnp.float32)]
    ppermute x2 -> x0, starting transfers between devices: 8.26 us -> none  [passed_along(): return lax.ppermute(block, axis, route)]
    pallas_call x2 -> x1, Pallas kernels: 130 us -> 123 us  [shards(): pl.pallas_call(functools.partial(layer_kernel, n_sp, nz, cap), out_shape=...]
  transfers between devices with their start and end apart: 2 -> 0, of which waited for: 0 -> 0; matrix products, arithmetic and copies ran while one was open for 4% -> 0% of each run, Pallas kernels for 0% -> 0%
where the time goes in v2:
time: 130 us; the launch traced here: 129 us
  Pallas kernels  123 us (95%)
  local copies, waits for them, and re-layouts  3.79 us (3%)
  other arithmetic  2.63 us (2%)
    pallas_call x1, Pallas kernels, shards(): pl.pallas_call(functools.partial(layer_kernel, n_sp, nz, cap), out_shape=...  123 us

profile of v2, /device:TPU:0, one launch (start us, length us, event | category | flops | bytes accessed | tf_op | source)
XLA Modules:
  0.0 129.4 jit_solution(9341666145854475861)
XLA Ops:
  0.0 0.7 convert_bitcast_fusion
  0.7 1.3 pad_maximum_fusion.routes
  1.9 0.7 convert_element_type.6
  2.6 1.3 broadcast_in_dim.10.gain
  3.9 0.8 broadcast_in_dim.4.docs
  4.7 122.9 %shard_map.127 = bf16[64,2048]{1,0:T(8,128)(2,1)} custom-call(bf16[512,256]{1,0:T(8,128)(2,1)} %in_gate.1, bf16[512,256]{1,0:T(8,128)(2,1)} %conv_input.1, bf16[512,256]{1,0:T(8,128)(2,1)} %out_gate.1, bf16[3,256]{1,0:T(4,128)(2,1)} %taps.1, f32[512,128]{1,0:T(8,128)} %broadcast_in_dim.4.docs, bf16[256,2048]{1,0:T(8,128)(2,1)} %out_weight.1, ...), custom_call_target="tpu_custom_call" | custom-call | tf_op jit(solution)/shard_map/pallas_call | solution.py:361
  127.7 1.7 %copy.15 = bf16[64,2048]{1,0:T(8,128)(2,1)} copy(bf16[64,2048]{1,0:T(8,128)(2,1)} %shard_map.127) | data formatting | bytes 524288
